TPU v7x, 32 devices: a whole 2x2x4 slice. The times are simulated.
32 devices in a mesh: fs: 8 (over z, x), tp: 4 (over y, core).
Axes of the slice: x: 2, y: 2, z: 4, core: 2. Of those that a mesh axis runs over, the one named last changes fastest.
Arguments:
- tokens: bfloat16 [6144, 2048], P('fs', 'tp'), may hold values from -6 to 6
- ffn_one_gain: float32 [2048], replicated, may hold values from 0.1 to 1.9
- ffn_one_gate: bfloat16 [2048, 5632], P('fs', 'tp'), may hold values from -0.125 to 0.125
- ffn_one_up: bfloat16 [2048, 5632], P('fs', 'tp'), may hold values from -0.125 to 0.125
- ffn_one_down: bfloat16 [5632, 2048], P('tp', 'fs'), may hold values from -0.078125 to 0.078125
- mix_gain: float32 [2048], replicated, may hold values from 0.1 to 1.9
- conv_value: bfloat16 [2048, 1024], P('fs', 'tp'), may hold values from -0.125 to 0.125
- conv_gate: bfloat16 [2048, 1024], P('fs', 'tp'), may hold values from -0.125 to 0.125
- conv_kernel: float32 [31, 1024], P(None, 'tp'), may hold values from -15 to 15
- conv_ln_gain: float32 [1024], P('tp'), may hold values from 0.1 to 1.9
- conv_out: bfloat16 [1024, 2048], P('tp', 'fs'), may hold values from -0.1875 to 0.1875
- ffn_two_gain: float32 [2048], replicated, may hold values from 0.1 to 1.9
- ffn_two_gate: bfloat16 [2048, 5632], P('fs', 'tp'), may hold values from -0.125 to 0.125
- ffn_two_up: bfloat16 [2048, 5632], P('fs', 'tp'), may hold values from -0.125 to 0.125
- ffn_two_down: bfloat16 [5632, 2048], P('tp', 'fs'), may hold values from -0.078125 to 0.078125
Outputs:
- layer_out: bfloat16 [6144, 2048], P('fs', 'tp')
All inputs are finite; a program needn't handle non-finite values.
Results may differ from a plain program's by a relative error of at most 0.017.
Values may be sent and summed in bfloat16 or wider, within the bound.
A program may use at most 128 MiB of HBM per device.

v0:
```python
from functools import partial
import jax
import jax.numpy as jnp
from jax import lax
from jax.sharding import PartitionSpec as P

CONV = 1024


def rms_rows(rows_in, gain_vec):
    values = rows_in.astype(jnp.float32)
    scaled = (
        values * lax.rsqrt(jnp.mean(values * values, axis=-1, keepdims=True) + 1e-06) * gain_vec
    )
    return scaled.astype(jnp.bfloat16)


def add_one(normed, running, shard_piece):
    columns = lax.slice_in_dim(normed, 0, shard_piece.shape[0], axis=1)
    return running + jnp.dot(columns, shard_piece, preferred_element_type=jnp.float32)


def add_two(normed, pieces):
    return (
        jnp.dot(normed, pieces[0], preferred_element_type=jnp.float32),
        jnp.dot(normed, pieces[1], preferred_element_type=jnp.float32),
    )


def ffn_terms(full_rows, gain_vec, w_gate, w_up, w_down):
    normed = rms_rows(full_rows, gain_vec)
    zero_carry = jnp.zeros((normed.shape[0], w_gate.shape[1]), jnp.float32)
    gate_pre = add_one(normed, zero_carry, lax.all_gather(w_gate, "fs", axis=0, tiled=True))
    up_pre = add_one(normed, zero_carry, lax.all_gather(w_up, "fs", axis=0, tiled=True))
    hidden = (jax.nn.silu(gate_pre) * up_pre).astype(jnp.bfloat16)
    return jnp.dot(
        hidden, lax.all_gather(w_down, "fs", axis=1, tiled=True), preferred_element_type=jnp.float32
    )


def conv_terms(full_rows, mix_gain, conv_value, conv_gate, conv_kernel, conv_ln_gain, conv_out):
    normed = rms_rows(full_rows, mix_gain)
    value_pre, gate_pre = add_two(
        normed,
        (
            lax.all_gather(conv_value, "fs", axis=0, tiled=True),
            lax.all_gather(conv_gate, "fs", axis=0, tiled=True),
        ),
    )
    gated_lin = value_pre * jax.nn.sigmoid(gate_pre)
    half_span = conv_kernel.shape[0] // 2
    convolved = lax.conv_general_dilated(
        gated_lin[None],
        conv_kernel[:, None, :],
        (1,),
        [(half_span, half_span)],
        dimension_numbers=("NWC", "WIO", "NWC"),
        feature_group_count=gated_lin.shape[1],
        precision=lax.Precision.HIGHEST,
    )[0]
    sum_one, sum_two = lax.psum(
        (jnp.sum(convolved, axis=1), jnp.sum(convolved * convolved, axis=1)), "tp"
    )
    mean_val = (sum_one / CONV)[:, None]
    varied = (sum_two / CONV)[:, None] - mean_val * mean_val
    active = jax.nn.silu((convolved - mean_val) * lax.rsqrt(varied + 1e-05) * conv_ln_gain).astype(
        jnp.bfloat16
    )
    return jnp.dot(
        active,
        lax.all_gather(conv_out, "fs", axis=1, tiled=True),
        preferred_element_type=jnp.float32,
    )


def per_device(
    tokens,
    ffn_one_gain,
    ffn_one_gate,
    ffn_one_up,
    ffn_one_down,
    mix_gain,
    conv_value,
    conv_gate,
    conv_kernel,
    conv_ln_gain,
    conv_out,
    ffn_two_gain,
    ffn_two_gate,
    ffn_two_up,
    ffn_two_down,
):
    sublayers = [
        (
            partial(
                ffn_terms,
                gain_vec=ffn_one_gain,
                w_gate=ffn_one_gate,
                w_up=ffn_one_up,
                w_down=ffn_one_down,
            ),
            0.5,
        ),
        (
            partial(
                conv_terms,
                mix_gain=mix_gain,
                conv_value=conv_value,
                conv_gate=conv_gate,
                conv_kernel=conv_kernel,
                conv_ln_gain=conv_ln_gain,
                conv_out=conv_out,
            ),
            1.0,
        ),
        (
            partial(
                ffn_terms,
                gain_vec=ffn_two_gain,
                w_gate=ffn_two_gate,
                w_up=ffn_two_up,
                w_down=ffn_two_down,
            ),
            0.5,
        ),
    ]
    current = tokens
    for sublayer, factor in sublayers:
        full_rows = lax.all_gather(current, "tp", axis=1, tiled=True)
        summed = lax.psum_scatter(
            sublayer(full_rows).astype(jnp.bfloat16), "tp", scatter_dimension=1, tiled=True
        ).astype(jnp.float32)
        current = (current.astype(jnp.float32) + factor * summed).astype(jnp.bfloat16)
    return current


def solution(mesh):
    in_specs = (
        P("fs", "tp"),
        P(),
        P("fs", "tp"),
        P("fs", "tp"),
        P("tp", "fs"),
        P(),
        P("fs", "tp"),
        P("fs", "tp"),
        P(None, "tp"),
        P("tp"),
        P("tp", "fs"),
        P(),
        P("fs", "tp"),
        P("fs", "tp"),
        P("tp", "fs"),
    )
    out_specs = P("fs", "tp")
    return jax.shard_map(
        per_device, mesh=mesh, in_specs=in_specs, out_specs=out_specs, check_vma=False
    )
```

profile of v0, /device:TPU:0, one launch (start us, length us, event | category | flops | bytes accessed | tf_op | source)
XLA Modules:
  0.0 943.1 jit_solution(7540141789120171966)
XLA Ops:
  6.5 0.7 all-gather.13.cloned.1.call-update
  9.4 30.8 %all-gather.13.cloned.1.call-done = bf16[768,2048]{1,0:T(8,128)(2,1)} async-done(((bf16[768,512]{1,0:T(8,128)(2,1)}), bf16[768,2048]{1,0:T(8,128)(2,1)}) %all-gather.13.cloned.1.call-update) | async-done | bytes 3145744 | tf_op jit(solution)/shard_map/all_gather | solution.py:129
  40.2 2.6 fusion
  42.8 91.9 %all-gather.15.cloned.1.call-done = bf16[2048,1408]{1,0:T(8,128)(2,1)} async-done(((bf16[256,1408]{1,0:T(8,128)(2,1)}), bf16[2048,1408]{1,0:T(8,128)(2,1)}) %all-gather.15.cloned.1.call-update) | async-done | bytes 5767184 | tf_op jit(solution)/shard_map/all_gather | solution.py:33
  134.7 9.9 %fusion.23 = f32[768,1408]{1,0:T(8,128)} fusion(bf16[2048,1408]{1,0:T(8,128)(2,1)} %all-gather.15.cloned.1.call-done, bf16[768,2048]{1,0:T(8,128)(2,1)} %all-gather.13.cloned.1.call-done, f32[2048]{0:T(1024)S(1)} %copy-done.6, f32[768]{0:T(1024)S(1)} %add_rsqrt_fusion.3), kind=kOutput, calls=%fused_computation.36 | convolution fusion | flops 4435476480 | bytes 13249536 | tf_op jit(solution)/shard_map/dot_general | solution.py:20
  144.6 82.8 %all-gather.17.cloned.1.call-done = bf16[2048,1408]{1,0:T(8,128)(2,1)} async-done(((bf16[256,1408]{1,0:T(8,128)(2,1)}), bf16[2048,1408]{1,0:T(8,128)(2,1)}) %all-gather.17.cloned.1.call-update) | async-done | bytes 5767184 | tf_op jit(solution)/shard_map/all_gather | solution.py:34
  227.4 93.2 %all-gather.19.cloned.1.call-done = bf16[1408,2048]{1,0:T(8,128)(2,1)} async-done(((bf16[1408,256]{1,0:T(8,128)(2,1)}), bf16[1408,2048]{1,0:T(8,128)(2,1)}) %all-gather.19.cloned.1.call-update) | async-done | bytes 5767184 | tf_op jit(solution)/shard_map/all_gather | solution.py:37
  320.6 17.4 %convolution_convert_fusion.2 = bf16[768,2048]{1,0:T(8,128)(2,1)} fusion(bf16[1408,2048]{1,0:T(8,128)(2,1)} %all-gather.19.cloned.1.call-done, f32[768,1408]{1,0:T(8,128)} %fusion.23, bf16[2048,1408]{1,0:T(8,128)(2,1)} %all-gather.17.cloned.1.call-done, bf16[768,2048]{1,0:T(8,128)(2,1)S(1)} %copy-done.4, f32[2048]{0:T(1024)S(1)} %copy-done.6, ...), kind=kOutput, calls=%fused_computation.19 | convolution fusion | flops 8872722432 | bytes 22162432 | tf_op jit(solution)/shard_map/dot_general | solution.py:36
  338.1 36.0 %reduce-scatter.4.cloned.1.call-done = bf16[768,512]{1,0:T(8,128)(2,1)} async-done(((bf16[768,2048]{1,0:T(8,128)(2,1)}), bf16[768,512]{1,0:T(8,128)(2,1)}) %reduce-scatter.4.cloned.1.call-update) | async-done | bytes 786448 | tf_op jit(solution)/shard_map/reduce_scatter | solution.py:130
  374.1 2.5 add_convert_fusion.2
  376.6 0.7 all-gather.25.cloned.1.call-update
  379.0 26.2 %all-gather.21.cloned.1.call-done = bf16[768,2048]{1,0:T(8,128)(2,1)} async-done(((bf16[768,512]{1,0:T(8,128)(2,1)}), bf16[768,2048]{1,0:T(8,128)(2,1)}) %all-gather.21.cloned.1.call-update) | async-done | bytes 3145744 | tf_op jit(solution)/shard_map/all_gather | solution.py:129
  405.2 2.6 fusion.3
  407.8 39.8 %all-gather.25.cloned.1.call-done = bf16[2048,256]{1,0:T(8,128)(2,1)} async-done(((bf16[256,256]{1,0:T(8,128)(2,1)}), bf16[2048,256]{1,0:T(8,128)(2,1)}) %all-gather.25.cloned.1.call-update) | async-done | bytes 1048592 | tf_op jit(solution)/shard_map/all_gather | solution.py:47
  447.7 4.1 fusion.12
  451.8 37.0 %all-gather.23.cloned.1.call-done = bf16[2048,256]{1,0:T(8,128)(2,1)} async-done(((bf16[256,256]{1,0:T(8,128)(2,1)}), bf16[2048,256]{1,0:T(8,128)(2,1)}) %all-gather.23.cloned.1.call-update) | async-done | bytes 1048592 | tf_op jit(solution)/shard_map/all_gather | solution.py:46
  488.8 2.5 fusion.10
  492.0 1.7 convolution_select_fusion
  494.5 5.8 all-reduce
  500.3 28.7 %all-gather.27.cloned.1.call-done = bf16[256,2048]{1,0:T(8,128)(2,1)} async-done(((bf16[256,256]{1,0:T(8,128)(2,1)}), bf16[256,2048]{1,0:T(8,128)(2,1)}) %all-gather.27.cloned.1.call-update) | async-done | bytes 1048592 | tf_op jit(solution)/shard_map/all_gather | solution.py:71
  529.0 4.0 convolution_convert_fusion
  533.1 36.8 %reduce-scatter.6.cloned.1.call-done = bf16[768,512]{1,0:T(8,128)(2,1)} async-done(((bf16[768,2048]{1,0:T(8,128)(2,1)}), bf16[768,512]{1,0:T(8,128)(2,1)}) %reduce-scatter.6.cloned.1.call-update) | async-done | bytes 786448 | tf_op jit(solution)/shard_map/reduce_scatter | solution.py:130
  570.0 2.2 add_convert_fusion.1
  574.4 26.5 %all-gather.29.cloned.1.call-done = bf16[768,2048]{1,0:T(8,128)(2,1)} async-done(((bf16[768,512]{1,0:T(8,128)(2,1)}), bf16[768,2048]{1,0:T(8,128)(2,1)}) %all-gather.29.cloned.1.call-update) | async-done | bytes 3145744 | tf_op jit(solution)/shard_map/all_gather | solution.py:129
  600.9 2.6 fusion.6
  603.5 91.8 %all-gather.31.cloned.1.call-done = bf16[2048,1408]{1,0:T(8,128)(2,1)} async-done(((bf16[256,1408]{1,0:T(8,128)(2,1)}), bf16[2048,1408]{1,0:T(8,128)(2,1)}) %all-gather.31.cloned.1.call-update) | async-done | bytes 5767184 | tf_op jit(solution)/shard_map/all_gather | solution.py:33
  695.3 9.9 %fusion.18 = f32[768,1408]{1,0:T(8,128)} fusion(bf16[2048,1408]{1,0:T(8,128)(2,1)} %all-gather.31.cloned.1.call-done, bf16[768,2048]{1,0:T(8,128)(2,1)} %all-gather.29.cloned.1.call-done, f32[2048]{0:T(1024)S(1)} %copy-done.8, f32[768]{0:T(1024)S(1)} %add_rsqrt_fusion), kind=kOutput, calls=%fused_computation.35 | convolution fusion | flops 4435476480 | bytes 13249536 | tf_op jit(solution)/shard_map/dot_general | solution.py:20
  705.2 82.8 %all-gather.33.cloned.1.call-done = bf16[2048,1408]{1,0:T(8,128)(2,1)} async-done(((bf16[256,1408]{1,0:T(8,128)(2,1)}), bf16[2048,1408]{1,0:T(8,128)(2,1)}) %all-gather.33.cloned.1.call-update) | async-done | bytes 5767184 | tf_op jit(solution)/shard_map/all_gather | solution.py:34
  788.0 93.2 %all-gather.35.cloned.1.call-done = bf16[1408,2048]{1,0:T(8,128)(2,1)} async-done(((bf16[1408,256]{1,0:T(8,128)(2,1)}), bf16[1408,2048]{1,0:T(8,128)(2,1)}) %all-gather.35.cloned.1.call-update) | async-done | bytes 5767184 | tf_op jit(solution)/shard_map/all_gather | solution.py:37
  881.2 17.0 %convolution_convert_fusion.1 = bf16[768,2048]{1,0:T(8,128)(2,1)} fusion(bf16[1408,2048]{1,0:T(8,128)(2,1)} %all-gather.35.cloned.1.call-done, f32[768,1408]{1,0:T(8,128)} %fusion.18, bf16[2048,1408]{1,0:T(8,128)(2,1)} %all-gather.33.cloned.1.call-done, bf16[768,2048]{1,0:T(8,128)(2,1)} %all-gather.29.cloned.1.call-done, f32[2048]{0:T(1024)S(1)} %copy-done.8, ...), kind=kOutput, calls=%fused_computation.18 | convolution fusion | flops 8872722432 | bytes 22162432 | tf_op jit(solution)/shard_map/dot_general | solution.py:36
  898.2 36.1 %reduce-scatter.8.cloned.1.call-done = bf16[768,512]{1,0:T(8,128)(2,1)} async-done(((bf16[768,2048]{1,0:T(8,128)(2,1)}), bf16[768,512]{1,0:T(8,128)(2,1)}) %reduce-scatter.8.cloned.1.call-update) | async-done | bytes 786448 | tf_op jit(solution)/shard_map/reduce_scatter | solution.py:130
  934.3 2.2 add_convert_fusion
  (62 shorter events, 7.5 us)
Async XLA Ops:
  6.5 485.3 %copy-start = (f32[31,256]{1,0:T(8,128)S(1)}, f32[31,256]{1,0:T(8,128)}, u32[]{:S(2)}) copy-start(f32[31,256]{1,0:T(8,128)} %param.23) | copy-start | bytes 95236
  6.5 128.1 %copy-start.6 = (f32[2048]{0:T(1024)S(1)}, f32[2048]{0:T(1024)}, u32[]{:S(2)}) copy-start(f32[2048]{0:T(1024)} %param.16) | copy-start | bytes 24580
  6.5 33.6 %all-gather.13.cloned.1.call-start = ((), (), s32[]{:S(2)}) async-start(), calls=%async_computation.3 | async-start | bytes 3932160 | tf_op jit(solution)/shard_map/all_gather | solution.py:129
  7.3 127.4 %all-gather.15.cloned.1.call-start = ((), (), s32[]{:S(2)}) async-start(), calls=%async_computation.4 | async-start | bytes 6488064 | tf_op jit(solution)/shard_map/all_gather | solution.py:33
  8.0 219.4 %all-gather.17.cloned.1.call-start = ((), (), s32[]{:S(2)}) async-start(), calls=%async_computation.5 | async-start | bytes 6488064 | tf_op jit(solution)/shard_map/all_gather | solution.py:34
  8.7 311.9 %all-gather.19.cloned.1.call-start = ((), (), s32[]{:S(2)}) async-start(), calls=%async_computation.6 | async-start | bytes 6488064 | tf_op jit(solution)/shard_map/all_gather | solution.py:37
  9.3 364.8 %reduce-scatter.4.cloned.1.call-start = ((), (), s32[]{:S(2)}) async-start(), calls=%async_computation.7 | async-start | bytes 3932160 | tf_op jit(solution)/shard_map/reduce_scatter | solution.py:130
  42.7 277.9 %copy-start.4 = (bf16[768,2048]{1,0:T(8,128)(2,1)S(1)}, bf16[768,2048]{1,0:T(8,128)(2,1)}, u32[]{:S(2)}) copy-start(bf16[768,2048]{1,0:T(8,128)(2,1)} %all-gather.13.cloned.1.call-done) | copy-start | bytes 9437188
  338.0 109.7 %copy-start.7 = (f32[2048]{0:T(1024)S(1)}, f32[2048]{0:T(1024)}, u32[]{:S(2)}) copy-start(f32[2048]{0:T(1024)} %param.20) | copy-start | bytes 24580
  338.0 67.2 %all-gather.21.cloned.1.call-start = ((), (), s32[]{:S(2)}) async-start(), calls=%async_computation.8 | async-start | bytes 3932160 | tf_op jit(solution)/shard_map/all_gather | solution.py:129
  376.6 71.1 %all-gather.25.cloned.1.call-start = ((), (), s32[]{:S(2)}) async-start(), calls=%async_computation.10 | async-start | bytes 1179648 | tf_op jit(solution)/shard_map/all_gather | solution.py:47
  377.3 111.5 %all-gather.23.cloned.1.call-start = ((), (), s32[]{:S(2)}) async-start(), calls=%async_computation.9 | async-start | bytes 1179648 | tf_op jit(solution)/shard_map/all_gather | solution.py:46
  378.1 150.9 %all-gather.27.cloned.1.call-start = ((), (), s32[]{:S(2)}) async-start(), calls=%async_computation.11 | async-start | bytes 1179648 | tf_op jit(solution)/shard_map/all_gather | solution.py:71
  378.8 191.1 %reduce-scatter.6.cloned.1.call-start = ((), (), s32[]{:S(2)}) async-start(), calls=%async_computation.12 | async-start | bytes 3932160 | tf_op jit(solution)/shard_map/reduce_scatter | solution.py:130
  407.8 81.0 %copy-start.5 = (bf16[768,2048]{1,0:T(8,128)(2,1)S(1)}, bf16[768,2048]{1,0:T(8,128)(2,1)}, u32[]{:S(2)}) copy-start(bf16[768,2048]{1,0:T(8,128)(2,1)} %all-gather.21.cloned.1.call-done) | copy-start | bytes 9437188
  491.3 0.7 copy-start.10
  493.8 35.3 %copy-start.9 = (f32[256]{0:T(256)S(1)}, f32[256]{0:T(256)}, u32[]{:S(2)}) copy-start(f32[256]{0:T(256)} %param.24) | copy-start | bytes 3076
  529.0 40.9 %copy-start.2 = (bf16[768,512]{1,0:T(8,128)(2,1)S(1)}, bf16[768,512]{1,0:T(8,128)(2,1)}, u32[]{:S(2)}) copy-start(bf16[768,512]{1,0:T(8,128)(2,1)} %add_convert_fusion.2) | copy-start | bytes 2359300
  533.1 162.2 %copy-start.8 = (f32[2048]{0:T(1024)S(1)}, f32[2048]{0:T(1024)}, u32[]{:S(2)}) copy-start(f32[2048]{0:T(1024)} %param.26) | copy-start | bytes 24580
  533.1 67.8 %all-gather.29.cloned.1.call-start = ((), (), s32[]{:S(2)}) async-start(), calls=%async_computation.13 | async-start | bytes 3932160 | tf_op jit(solution)/shard_map/all_gather | solution.py:129
  572.2 123.0 %all-gather.31.cloned.1.call-start = ((), (), s32[]{:S(2)}) async-start(), calls=%async_computation.14 | async-start | bytes 6488064 | tf_op jit(solution)/shard_map/all_gather | solution.py:33
  572.8 215.2 %all-gather.33.cloned.1.call-start = ((), (), s32[]{:S(2)}) async-start(), calls=%async_computation.15 | async-start | bytes 6488064 | tf_op jit(solution)/shard_map/all_gather | solution.py:34
  573.5 307.7 %all-gather.35.cloned.1.call-start = ((), (), s32[]{:S(2)}) async-start(), calls=%async_computation.16 | async-start | bytes 6488064 | tf_op jit(solution)/shard_map/all_gather | solution.py:37
  574.1 360.2 %reduce-scatter.8.cloned.1.call-start = ((), (), s32[]{:S(2)}) async-start(), calls=%async_computation.17 | async-start | bytes 3932160 | tf_op jit(solution)/shard_map/reduce_scatter | solution.py:130
  705.2 229.1 %copy-start.3 = (bf16[768,512]{1,0:T(8,128)(2,1)S(1)}, bf16[768,512]{1,0:T(8,128)(2,1)}, u32[]{:S(2)}) copy-start(bf16[768,512]{1,0:T(8,128)(2,1)} %add_convert_fusion.1) | copy-start | bytes 2359300
  881.2 55.3 %copy-start.1 = (f32[31,256]{1,0:T(8,128)S(1)}, f32[31,256]{1,0:T(8,128)}, u32[]{:S(2)}) copy-start(f32[31,256]{1,0:T(8,128)} %param.23) | copy-start | bytes 95236
Sparse Core Ops, SparseCore 0:
  8.9 31.2 all-gather.12
  42.3 92.2 all-gather.14
  136.9 90.4 all-gather.16
  229.3 91.2 all-gather.18
  338.1 35.8 reduce-scatter.3
  376.7 28.4 all-gather.20
  407.4 40.2 all-gather.24
  449.8 38.9 all-gather.22
  490.9 38.0 all-gather.26
  533.2 36.7 reduce-scatter.5
  572.3 28.5 all-gather.28
  602.9 92.2 all-gather.30
  697.4 90.4 all-gather.32
  789.9 91.2 all-gather.34
  898.3 35.9 reduce-scatter.7
where the time goes:
time: 944 us; the launch traced here: 943 us
  waiting for transfers between devices  840 us (89%)
  matrix products  66.6 us (7%)
  other arithmetic  15 us (2%)
  between operations  13.5 us (1%)
    all_gather x2, waiting for transfers between devices, ffn_terms(): lax.all_gather(w_down, 'fs', axis=1, tiled=True)  186 us
    all_gather x2, waiting for transfers between devices, ffn_terms(): lax.all_gather(w_gate, 'fs', axis=0, tiled=True)  184 us
    all_gather x2, waiting for transfers between devices, ffn_terms(): lax.all_gather(w_up, 'fs', axis=0, tiled=True)  166 us
    reduce_scatter x3, waiting for transfers between devices, per_device(): lax.psum_scatter(sublayer(full_rows).astype(jnp.bfloat16), 'tp', scatter_...  109 us
    all_gather x3, waiting for transfers between devices, per_device(): full_rows = lax.all_gather(current, 'tp', axis=1, tiled=True)  83.5 us
    all_gather x1, waiting for transfers between devices, conv_terms(): lax.all_gather(conv_gate, 'fs', axis=0, tiled=True)  39.8 us
    all_gather x1, waiting for transfers between devices, conv_terms(): lax.all_gather(conv_value, 'fs', axis=0, tiled=True)  37 us
    dot_general x2, matrix products, ffn_terms(): jnp.dot(hidden, lax.all_gather(w_down, 'fs', axis=1, tiled=True), preferr...  34.3 us
  transfers between devices with their start and end apart: 15, of which 15 were waited for; matrix products, arithmetic and copies ran while one was open for 4% of the time, Pallas kernels for 0%

commit v1 on v0

--- a/solution.py
+++ b/solution.py
@@ -126,7 +126,14 @@
     ]
     current = tokens
     for sublayer, factor in sublayers:
-        full_rows = lax.all_gather(current, "tp", axis=1, tiled=True)
+        ring = [current]
+        for hop in range(3):
+            ring.append(lax.ppermute(ring[-1], "tp", [(dev, (dev + 1) % 4) for dev in range(4)]))
+        full_rows = jnp.roll(
+            jnp.concatenate(ring[::-1], axis=1),
+            (lax.axis_index("tp") + 1) * ring[0].shape[1],
+            axis=1,
+        )
         summed = lax.psum_scatter(
             sublayer(full_rows).astype(jnp.bfloat16), "tp", scatter_dimension=1, tiled=True
         ).astype(jnp.float32)

time: 944 us -> 851 us (0.901)
  waiting for transfers between devices: 840 us -> 729 us
  other arithmetic: 15 us -> 32.4 us
    ppermute x0 -> x9, waiting for transfers between devices: none -> 102 us  [per_device(): lax.ppermute(ring[-1], 'tp', [(dev, (dev + 1) % 4) for dev in range(4)])]
    all_gather x3 -> x0, waiting for transfers between devices: 83.5 us -> none  [per_device(): full_rows = lax.all_gather(current, 'tp', axis=1, tiled=True)]
    all_gather x2, waiting for transfers between devices: 184 us -> 101 us  [ffn_terms(): lax.all_gather(w_gate, 'fs', axis=0, tiled=True)]
    all_gather x1, waiting for transfers between devices: 39.8 us -> 0.01 us  [conv_terms(): lax.all_gather(conv_gate, 'fs', axis=0, tiled=True)]
    reduce_sum x3, other arithmetic: 7.71 us -> 26.8 us  [rms_rows(): jnp.mean(values * values, axis=-1, keepdims=True) + 1e-06]
  transfers between devices with their start and end apart: 15 -> 21, of which waited for: 15 -> 20; matrix products, arithmetic and copies ran while one was open for 4% -> 7% of each run, Pallas kernels for 0% -> 0%
where the time goes in v1:
time: 851 us
  waiting for transfers between devices  729 us (86%)
  matrix products  65.8 us (8%)
  other arithmetic  32.4 us (4%)
  between operations  13.8 us (2%)
    all_gather x2, waiting for transfers between devices, ffn_terms(): lax.all_gather(w_down, 'fs', axis=1, tiled=True)  187 us
    all_gather x2, waiting for transfers between devices, ffn_terms(): lax.all_gather(w_up, 'fs', axis=0, tiled=True)  166 us
    reduce_scatter x3, waiting for transfers between devices, per_device(): lax.psum_scatter(sublayer(full_rows).astype(jnp.bfloat16), 'tp', scatter_...  106 us
    ppermute x9, waiting for transfers between devices, per_device(): lax.ppermute(ring[-1], 'tp', [(dev, (dev + 1) % 4) for dev in range(4)])  102 us
    all_gather x2, waiting for transfers between devices, ffn_terms(): lax.all_gather(w_gate, 'fs', axis=0, tiled=True)  101 us
    all_gather x1, waiting for transfers between devices, conv_terms(): lax.all_gather(conv_value, 'fs', axis=0, tiled=True)  34.6 us
    dot_general x2, matrix products, ffn_terms(): jnp.dot(hidden, lax.all_gather(w_down, 'fs', axis=1, tiled=True), preferr...  34.3 us
    all_gather x1, waiting for transfers between devices, conv_terms(): lax.all_gather(conv_out, 'fs', axis=1, tiled=True)  28.2 us
  transfers between devices with their start and end apart: 21, of which 20 were waited for; matrix products, arithmetic and copies ran while one was open for 7% of the time, Pallas kernels for 0%

profile of v1, /device:TPU:0, one launch (start us, length us, event | category | flops | bytes accessed | tf_op | source)
XLA Modules:
  0.0 851.1 jit_solution(9008660202588296007)
XLA Ops:
  9.3 11.8 %collective-permute-done = bf16[768,512]{1,0:T(8,128)(2,1)S(1)} collective-permute-done((bf16[768,512]{1,0:T(8,128)(2,1)}, bf16[768,512]{1,0:T(8,128)(2,1)S(1)}, u32[]{:S(2)}, u32[]{:S(2)}) %collective-permute-start) | collective-permute-done | bytes 786464 | tf_op jit(solution)/shard_map/ppermute | solution.py:131
  22.1 11.4 %collective-permute-done.1 = bf16[768,512]{1,0:T(8,128)(2,1)S(1)} collective-permute-done((bf16[768,512]{1,0:T(8,128)(2,1)S(1)}, bf16[768,512]{1,0:T(8,128)(2,1)S(1)}, u32[]{:S(2)}, u32[]{:S(2)}) %collective-permute-start.1) | collective-permute-done | bytes 786464 | tf_op jit(solution)/shard_map/ppermute | solution.py:131
  34.4 10.6 %collective-permute-done.2 = bf16[768,512]{1,0:T(8,128)(2,1)} collective-permute-done((bf16[768,512]{1,0:T(8,128)(2,1)S(1)}, bf16[768,512]{1,0:T(8,128)(2,1)}, u32[]{:S(2)}, u32[]{:S(2)}) %collective-permute-start.2) | collective-permute-done | bytes 786464 | tf_op jit(solution)/shard_map/ppermute | solution.py:131
  45.0 7.7 fusion
  52.7 51.8 %all-gather.10.cloned.1.call-done = bf16[2048,1408]{1,0:T(8,128)(2,1)} async-done(((bf16[256,1408]{1,0:T(8,128)(2,1)}), bf16[2048,1408]{1,0:T(8,128)(2,1)}) %all-gather.10.cloned.1.call-update) | async-done | bytes 5767184 | tf_op jit(solution)/shard_map/all_gather | solution.py:33
  104.6 9.4 %fusion.44 = f32[768,1408]{1,0:T(8,128)} fusion(bf16[2048,1408]{1,0:T(8,128)(2,1)} %all-gather.10.cloned.1.call-done, bf16[768,2048]{1,0:T(8,128)(2,1)S(1)} %get-tuple-element.13, f32[2048]{0:T(1024)S(1)} %copy-done.4, f32[768]{0:T(1024)S(1)} %add_rsqrt_fusion.3), kind=kOutput, calls=%fused_computation.81 | convolution fusion | flops 4435476480 | bytes 13249536 | tf_op jit(solution)/shard_map/dot_general | solution.py:20
  114.0 83.3 %all-gather.12.cloned.1.call-done = bf16[2048,1408]{1,0:T(8,128)(2,1)} async-done(((bf16[256,1408]{1,0:T(8,128)(2,1)}), bf16[2048,1408]{1,0:T(8,128)(2,1)}) %all-gather.12.cloned.1.call-update) | async-done | bytes 5767184 | tf_op jit(solution)/shard_map/all_gather | solution.py:34
  197.3 93.4 %all-gather.14.cloned.1.call-done = bf16[1408,2048]{1,0:T(8,128)(2,1)} async-done(((bf16[1408,256]{1,0:T(8,128)(2,1)}), bf16[1408,2048]{1,0:T(8,128)(2,1)}) %all-gather.14.cloned.1.call-update) | async-done | bytes 5767184 | tf_op jit(solution)/shard_map/all_gather | solution.py:37
  290.7 17.4 %convolution_convert_fusion.2 = bf16[768,2048]{1,0:T(8,128)(2,1)} fusion(bf16[1408,2048]{1,0:T(8,128)(2,1)} %all-gather.14.cloned.1.call-done, f32[768,1408]{1,0:T(8,128)} %fusion.44, bf16[2048,1408]{1,0:T(8,128)(2,1)} %all-gather.12.cloned.1.call-done, bf16[768,2048]{1,0:T(8,128)(2,1)S(1)} %get-tuple-element.13, f32[2048]{0:T(1024)S(1)} %copy-done.4, ...), kind=kOutput, calls=%fused_computation.43 | convolution fusion | flops 8872722432 | bytes 22162432 | tf_op jit(solution)/shard_map/dot_general | solution.py:36
  308.9 35.3 %reduce-scatter.4.cloned.1.call-done = bf16[768,512]{1,0:T(8,128)(2,1)} async-done(((bf16[768,2048]{1,0:T(8,128)(2,1)}), bf16[768,512]{1,0:T(8,128)(2,1)}) %reduce-scatter.4.cloned.1.call-update) | async-done | bytes 786448 | tf_op jit(solution)/shard_map/reduce_scatter | solution.py:137
  345.9 11.3 %collective-permute-done.3 = bf16[768,512]{1,0:T(8,128)(2,1)S(1)} collective-permute-done((bf16[768,512]{1,0:T(8,128)(2,1)S(1)}, bf16[768,512]{1,0:T(8,128)(2,1)S(1)}, u32[]{:S(2)}, u32[]{:S(2)}) %collective-permute-start.3) | collective-permute-done | bytes 786464 | tf_op jit(solution)/shard_map/ppermute | solution.py:131
  357.2 11.4 %collective-permute-done.4 = bf16[768,512]{1,0:T(8,128)(2,1)S(1)} collective-permute-done((bf16[768,512]{1,0:T(8,128)(2,1)S(1)}, bf16[768,512]{1,0:T(8,128)(2,1)S(1)}, u32[]{:S(2)}, u32[]{:S(2)}) %collective-permute-start.4) | collective-permute-done | bytes 786464 | tf_op jit(solution)/shard_map/ppermute | solution.py:131
  368.7 11.3 %collective-permute-done.5 = bf16[768,512]{1,0:T(8,128)(2,1)S(1)} collective-permute-done((bf16[768,512]{1,0:T(8,128)(2,1)S(1)}, bf16[768,512]{1,0:T(8,128)(2,1)S(1)}, u32[]{:S(2)}, u32[]{:S(2)}) %collective-permute-start.5) | collective-permute-done | bytes 786464 | tf_op jit(solution)/shard_map/ppermute | solution.py:131
  380.1 9.5 %fusion.3 = (f32[768]{0:T(1024)S(1)}, bf16[768,2048]{1,0:T(8,128)(2,1)}) fusion(s32[]{:T(128)S(6)} %select_n.15, bf16[768,512]{1,0:T(8,128)(2,1)S(1)} %add_convert_fusion.2, bf16[768,512]{1,0:T(8,128)(2,1)S(1)} %collective-permute-done.3, bf16[768,512]{1,0:T(8,128)(2,1)S(1)} %collective-permute-done.4, bf16[768,512]{1,0:T(8,128)(2,1)S(1)} %collective-permute-done.5), kind=kLoop, calls=%fused_computation.9 | loop fusion | flops 29883648 | bytes 6294532 | tf_op jit(solution)/shard_map/reduce_sum | solution.py:13
  389.6 3.2 fusion.33
  392.9 34.6 %all-gather.16.cloned.1.call-done = bf16[2048,256]{1,0:T(8,128)(2,1)} async-done(((bf16[256,256]{1,0:T(8,128)(2,1)}), bf16[2048,256]{1,0:T(8,128)(2,1)}) %all-gather.16.cloned.1.call-update) | async-done | bytes 1048592 | tf_op jit(solution)/shard_map/all_gather | solution.py:46
  427.4 3.2 fusion.31
  433.6 5.8 all-reduce
  439.4 28.2 %all-gather.20.cloned.1.call-done = bf16[256,2048]{1,0:T(8,128)(2,1)} async-done(((bf16[256,256]{1,0:T(8,128)(2,1)}), bf16[256,2048]{1,0:T(8,128)(2,1)}) %all-gather.20.cloned.1.call-update) | async-done | bytes 1048592 | tf_op jit(solution)/shard_map/all_gather | solution.py:71
  467.6 3.9 convolution_convert_fusion
  473.7 34.8 %reduce-scatter.6.cloned.1.call-done = bf16[768,512]{1,0:T(8,128)(2,1)} async-done(((bf16[768,2048]{1,0:T(8,128)(2,1)}), bf16[768,512]{1,0:T(8,128)(2,1)}) %reduce-scatter.6.cloned.1.call-update) | async-done | bytes 786448 | tf_op jit(solution)/shard_map/reduce_scatter | solution.py:137
  509.9 11.4 %collective-permute-done.6 = bf16[768,512]{1,0:T(8,128)(2,1)S(1)} collective-permute-done((bf16[768,512]{1,0:T(8,128)(2,1)S(1)}, bf16[768,512]{1,0:T(8,128)(2,1)S(1)}, u32[]{:S(2)}, u32[]{:S(2)}) %collective-permute-start.6) | collective-permute-done | bytes 786464 | tf_op jit(solution)/shard_map/ppermute | solution.py:131
  521.3 11.4 %collective-permute-done.7 = bf16[768,512]{1,0:T(8,128)(2,1)S(1)} collective-permute-done((bf16[768,512]{1,0:T(8,128)(2,1)S(1)}, bf16[768,512]{1,0:T(8,128)(2,1)S(1)}, u32[]{:S(2)}, u32[]{:S(2)}) %collective-permute-start.7) | collective-permute-done | bytes 786464 | tf_op jit(solution)/shard_map/ppermute | solution.py:131
  532.7 11.4 %collective-permute-done.8 = bf16[768,512]{1,0:T(8,128)(2,1)S(1)} collective-permute-done((bf16[768,512]{1,0:T(8,128)(2,1)S(1)}, bf16[768,512]{1,0:T(8,128)(2,1)S(1)}, u32[]{:S(2)}, u32[]{:S(2)}) %collective-permute-start.8) | collective-permute-done | bytes 786464 | tf_op jit(solution)/shard_map/ppermute | solution.py:131
  544.1 9.6 %fusion.6 = (f32[768]{0:T(1024)S(1)}, bf16[768,2048]{1,0:T(8,128)(2,1)}) fusion(s32[]{:T(128)S(6)} %select_n.15, bf16[768,512]{1,0:T(8,128)(2,1)S(1)} %add_convert_fusion.1, bf16[768,512]{1,0:T(8,128)(2,1)S(1)} %collective-permute-done.6, bf16[768,512]{1,0:T(8,128)(2,1)S(1)} %collective-permute-done.7, bf16[768,512]{1,0:T(8,128)(2,1)S(1)} %collective-permute-done.8), kind=kLoop, calls=%fused_computation.12 | loop fusion | flops 29883648 | bytes 6294532 | tf_op jit(solution)/shard_map/reduce_sum | solution.py:13
  553.7 49.3 %all-gather.22.cloned.1.call-done = bf16[2048,1408]{1,0:T(8,128)(2,1)} async-done(((bf16[256,1408]{1,0:T(8,128)(2,1)}), bf16[2048,1408]{1,0:T(8,128)(2,1)}) %all-gather.22.cloned.1.call-update) | async-done | bytes 5767184 | tf_op jit(solution)/shard_map/all_gather | solution.py:33
  603.0 9.9 %fusion.39 = f32[768,1408]{1,0:T(8,128)} fusion(bf16[2048,1408]{1,0:T(8,128)(2,1)} %all-gather.22.cloned.1.call-done, bf16[768,2048]{1,0:T(8,128)(2,1)} %get-tuple-element.9, f32[2048]{0:T(1024)S(1)} %copy-done.6, f32[768]{0:T(1024)S(1)} %add_rsqrt_fusion), kind=kOutput, calls=%fused_computation.80 | convolution fusion | flops 4435476480 | bytes 13249536 | tf_op jit(solution)/shard_map/dot_general | solution.py:20
  612.9 82.6 %all-gather.24.cloned.1.call-done = bf16[2048,1408]{1,0:T(8,128)(2,1)} async-done(((bf16[256,1408]{1,0:T(8,128)(2,1)}), bf16[2048,1408]{1,0:T(8,128)(2,1)}) %all-gather.24.cloned.1.call-update) | async-done | bytes 5767184 | tf_op jit(solution)/shard_map/all_gather | solution.py:34
  695.6 93.4 %all-gather.26.cloned.1.call-done = bf16[1408,2048]{1,0:T(8,128)(2,1)} async-done(((bf16[1408,256]{1,0:T(8,128)(2,1)}), bf16[1408,2048]{1,0:T(8,128)(2,1)}) %all-gather.26.cloned.1.call-update) | async-done | bytes 5767184 | tf_op jit(solution)/shard_map/all_gather | solution.py:37
  789.0 17.0 %convolution_convert_fusion.1 = bf16[768,2048]{1,0:T(8,128)(2,1)} fusion(bf16[1408,2048]{1,0:T(8,128)(2,1)} %all-gather.26.cloned.1.call-done, f32[768,1408]{1,0:T(8,128)} %fusion.39, bf16[2048,1408]{1,0:T(8,128)(2,1)} %all-gather.24.cloned.1.call-done, bf16[768,2048]{1,0:T(8,128)(2,1)} %get-tuple-element.9, f32[2048]{0:T(1024)S(1)} %copy-done.6, ...), kind=kOutput, calls=%fused_computation.42 | convolution fusion | flops 8872722432 | bytes 22162432 | tf_op jit(solution)/shard_map/dot_general | solution.py:36
  805.9 36.1 %reduce-scatter.8.cloned.1.call-done = bf16[768,512]{1,0:T(8,128)(2,1)} async-done(((bf16[768,2048]{1,0:T(8,128)(2,1)}), bf16[768,512]{1,0:T(8,128)(2,1)}) %reduce-scatter.8.cloned.1.call-update) | async-done | bytes 786448 | tf_op jit(solution)/shard_map/reduce_scatter | solution.py:137
  842.0 2.2 add_convert_fusion
  (67 shorter events, 13.6 us)
Async XLA Ops:
  6.5 424.6 %copy-start = (f32[31,256]{1,0:T(8,128)S(1)}, f32[31,256]{1,0:T(8,128)}, u32[]{:S(2)}) copy-start(f32[31,256]{1,0:T(8,128)} %param.25) | copy-start | bytes 95236
  6.5 98.0 %copy-start.4 = (f32[2048]{0:T(1024)S(1)}, f32[2048]{0:T(1024)}, u32[]{:S(2)}) copy-start(f32[2048]{0:T(1024)} %param.18) | copy-start | bytes 24580
  6.5 98.0 %all-gather.10.cloned.1.call-start = ((), (), s32[]{:S(2)}) async-start(), calls=%async_computation.3 | async-start | bytes 6488064 | tf_op jit(solution)/shard_map/all_gather | solution.py:33
  7.3 190.0 %all-gather.12.cloned.1.call-start = ((), (), s32[]{:S(2)}) async-start(), calls=%async_computation.4 | async-start | bytes 6488064 | tf_op jit(solution)/shard_map/all_gather | solution.py:34
  8.0 282.7 %all-gather.14.cloned.1.call-start = ((), (), s32[]{:S(2)}) async-start(), calls=%async_computation.5 | async-start | bytes 6488064 | tf_op jit(solution)/shard_map/all_gather | solution.py:37
  8.7 335.4 %reduce-scatter.4.cloned.1.call-start = ((), (), s32[]{:S(2)}) async-start(), calls=%async_computation.6 | async-start | bytes 3932160 | tf_op jit(solution)/shard_map/reduce_scatter | solution.py:137
  8.8 12.4 %collective-permute-start = (bf16[768,512]{1,0:T(8,128)(2,1)}, bf16[768,512]{1,0:T(8,128)(2,1)S(1)}, u32[]{:S(2)}, u32[]{:S(2)}) collective-permute-start(bf16[768,512]{1,0:T(8,128)(2,1)} %param.17), channel_id=1, source_target_pairs={{0,1},{1,2},{2,3},{3,0},{4,5},{5,6},{6,7},{7,4},{8,9},{9,10},{10,1... | collective-permute-start | bytes 2359304 | tf_op jit(solution)/shard_map/ppermute | solution.py:131
  21.2 0.9 copy-start.2
  22.0 11.4 %collective-permute-start.1 = (bf16[768,512]{1,0:T(8,128)(2,1)S(1)}, bf16[768,512]{1,0:T(8,128)(2,1)S(1)}, u32[]{:S(2)}, u32[]{:S(2)}) collective-permute-start(bf16[768,512]{1,0:T(8,128)(2,1)S(1)} %collective-permute-done), channel_id=1, source_target_pairs={{0,1},{1,2},{2,3},{3,0},{4,5},{5,6},{6,7},{7,4},{8,9},{9,10},{10,1... | collective-permute-start | bytes 2359304 | tf_op jit(solution)/shard_map/ppermute | solution.py:131
  33.5 0.9 copy-start.3
  33.5 11.5 %collective-permute-start.2 = (bf16[768,512]{1,0:T(8,128)(2,1)S(1)}, bf16[768,512]{1,0:T(8,128)(2,1)}, u32[]{:S(2)}, u32[]{:S(2)}) collective-permute-start(bf16[768,512]{1,0:T(8,128)(2,1)S(1)} %collective-permute-done.1), channel_id=1, source_target_pairs={{0,1},{1,2},{2,3},{3,0},{4,5},{5,6},{6,7},{7,4},{8,9},{9,10},{10,1... | collective-permute-start | bytes 2359304 | tf_op jit(solution)/shard_map/ppermute | solution.py:131
  308.0 81.6 %copy-start.5 = (f32[2048]{0:T(1024)S(1)}, f32[2048]{0:T(1024)}, u32[]{:S(2)}) copy-start(f32[2048]{0:T(1024)} %param.22) | copy-start | bytes 24580
  308.1 81.5 %all-gather.18.cloned.1.call-start = ((), (), s32[]{:S(2)}) async-start(), calls=%async_computation.8 | async-start | bytes 1179648 | tf_op jit(solution)/shard_map/all_gather | solution.py:47
  308.7 118.8 %all-gather.16.cloned.1.call-start = ((), (), s32[]{:S(2)}) async-start(), calls=%async_computation.7 | async-start | bytes 1179648 | tf_op jit(solution)/shard_map/all_gather | solution.py:46
  345.8 11.5 %collective-permute-start.3 = (bf16[768,512]{1,0:T(8,128)(2,1)S(1)}, bf16[768,512]{1,0:T(8,128)(2,1)S(1)}, u32[]{:S(2)}, u32[]{:S(2)}) collective-permute-start(bf16[768,512]{1,0:T(8,128)(2,1)S(1)} %add_convert_fusion.2), channel_id=1, source_target_pairs={{0,1},{1,2},{2,3},{3,0},{4,5},{5,6},{6,7},{7,4},{8,9},{9,10},{10,1... | collective-permute-start | bytes 2359304 | tf_op jit(solution)/shard_map/ppermute | solution.py:131
  345.8 121.8 %all-gather.20.cloned.1.call-start = ((), (), s32[]{:S(2)}) async-start(), calls=%async_computation.9 | async-start | bytes 1179648 | tf_op jit(solution)/shard_map/all_gather | solution.py:71
  357.2 11.4 %collective-permute-start.4 = (bf16[768,512]{1,0:T(8,128)(2,1)S(1)}, bf16[768,512]{1,0:T(8,128)(2,1)S(1)}, u32[]{:S(2)}, u32[]{:S(2)}) collective-permute-start(bf16[768,512]{1,0:T(8,128)(2,1)S(1)} %collective-permute-done.3), channel_id=1, source_target_pairs={{0,1},{1,2},{2,3},{3,0},{4,5},{5,6},{6,7},{7,4},{8,9},{9,10},{10,1... | collective-permute-start | bytes 2359304 | tf_op jit(solution)/shard_map/ppermute | solution.py:131
  368.6 11.4 %collective-permute-start.5 = (bf16[768,512]{1,0:T(8,128)(2,1)S(1)}, bf16[768,512]{1,0:T(8,128)(2,1)S(1)}, u32[]{:S(2)}, u32[]{:S(2)}) collective-permute-start(bf16[768,512]{1,0:T(8,128)(2,1)S(1)} %collective-permute-done.4), channel_id=1, source_target_pairs={{0,1},{1,2},{2,3},{3,0},{4,5},{5,6},{6,7},{7,4},{8,9},{9,10},{10,1... | collective-permute-start | bytes 2359304 | tf_op jit(solution)/shard_map/ppermute | solution.py:131
  368.7 139.8 %reduce-scatter.6.cloned.1.call-start = ((), (), s32[]{:S(2)}) async-start(), calls=%async_computation.10 | async-start | bytes 3932160 | tf_op jit(solution)/shard_map/reduce_scatter | solution.py:137
  392.9 38.3 %copy-start.8 = (pred[8,100]{0,1:T(8,128)(4,1)S(1)}, pred[8,100]{0,1:T(8,128)(4,1)}, u32[]{:S(2)}) copy-start(pred[8,100]{0,1:T(8,128)(4,1)} %constant.55) | copy-start | bytes 2404
  431.1 36.5 %copy-start.7 = (f32[256]{0:T(256)S(1)}, f32[256]{0:T(256)}, u32[]{:S(2)}) copy-start(f32[256]{0:T(256)} %param.26) | copy-start | bytes 3076
  471.6 131.4 %copy-start.6 = (f32[2048]{0:T(1024)S(1)}, f32[2048]{0:T(1024)}, u32[]{:S(2)}) copy-start(f32[2048]{0:T(1024)} %param.28) | copy-start | bytes 24580
  471.6 131.4 %all-gather.22.cloned.1.call-start = ((), (), s32[]{:S(2)}) async-start(), calls=%async_computation.11 | async-start | bytes 6488064 | tf_op jit(solution)/shard_map/all_gather | solution.py:33
  472.3 223.2 %all-gather.24.cloned.1.call-start = ((), (), s32[]{:S(2)}) async-start(), calls=%async_computation.12 | async-start | bytes 6488064 | tf_op jit(solution)/shard_map/all_gather | solution.py:34
  472.9 316.0 %all-gather.26.cloned.1.call-start = ((), (), s32[]{:S(2)}) async-start(), calls=%async_computation.13 | async-start | bytes 6488064 | tf_op jit(solution)/shard_map/all_gather | solution.py:37
  473.6 368.4 %reduce-scatter.8.cloned.1.call-start = ((), (), s32[]{:S(2)}) async-start(), calls=%async_computation.14 | async-start | bytes 3932160 | tf_op jit(solution)/shard_map/reduce_scatter | solution.py:137
  509.8 11.5 %collective-permute-start.6 = (bf16[768,512]{1,0:T(8,128)(2,1)S(1)}, bf16[768,512]{1,0:T(8,128)(2,1)S(1)}, u32[]{:S(2)}, u32[]{:S(2)}) collective-permute-start(bf16[768,512]{1,0:T(8,128)(2,1)S(1)} %add_convert_fusion.1), channel_id=1, source_target_pairs={{0,1},{1,2},{2,3},{3,0},{4,5},{5,6},{6,7},{7,4},{8,9},{9,10},{10,1... | collective-permute-start | bytes 2359304 | tf_op jit(solution)/shard_map/ppermute | solution.py:131
  521.3 11.4 %collective-permute-start.7 = (bf16[768,512]{1,0:T(8,128)(2,1)S(1)}, bf16[768,512]{1,0:T(8,128)(2,1)S(1)}, u32[]{:S(2)}, u32[]{:S(2)}) collective-permute-start(bf16[768,512]{1,0:T(8,128)(2,1)S(1)} %collective-permute-done.6), channel_id=1, source_target_pairs={{0,1},{1,2},{2,3},{3,0},{4,5},{5,6},{6,7},{7,4},{8,9},{9,10},{10,1... | collective-permute-start | bytes 2359304 | tf_op jit(solution)/shard_map/ppermute | solution.py:131
  532.7 11.4 %collective-permute-start.8 = (bf16[768,512]{1,0:T(8,128)(2,1)S(1)}, bf16[768,512]{1,0:T(8,128)(2,1)S(1)}, u32[]{:S(2)}, u32[]{:S(2)}) collective-permute-start(bf16[768,512]{1,0:T(8,128)(2,1)S(1)} %collective-permute-done.7), channel_id=1, source_target_pairs={{0,1},{1,2},{2,3},{3,0},{4,5},{5,6},{6,7},{7,4},{8,9},{9,10},{10,1... | collective-permute-start | bytes 2359304 | tf_op jit(solution)/shard_map/ppermute | solution.py:131
  789.0 55.3 %copy-start.1 = (f32[31,256]{1,0:T(8,128)S(1)}, f32[31,256]{1,0:T(8,128)}, u32[]{:S(2)}) copy-start(f32[31,256]{1,0:T(8,128)} %param.25) | copy-start | bytes 95236
Sparse Core Ops, SparseCore 0:
  9.5 95.0 all-gather.9
  106.8 90.4 all-gather.11
  199.3 91.2 all-gather.13
  308.2 35.9 reduce-scatter.3
  346.1 40.2 all-gather.17
  388.4 38.9 all-gather.15
  429.5 38.0 all-gather.19
  471.7 36.7 reduce-scatter.5
  510.7 92.2 all-gather.21
  605.0 90.4 all-gather.23
  697.6 91.2 all-gather.25
  806.1 35.9 reduce-scatter.7
